TPU v7x, 32 devices: a whole 2x2x4 slice. The times are simulated.
32 devices in a mesh: ep: 8 (over z, x), tp: 4 (over y, core).
Axes of the slice: x: 2, y: 2, z: 4, core: 2. Of those that a mesh axis runs over, the one named last changes fastest.
Arguments:
- tokens: bfloat16 [2048, 2048], P('ep')
- norm_gain: float32 [2048], replicated, may hold values from 0.1 to 1.9
- chosen: int32 [8, 256], replicated, may hold values from 0 to 2047, as said below
- route_weight: float32 [8, 256], P('ep'), may hold values from 0.2 to 1
- gate_weight: bfloat16 [8, 2048, 4096], P('ep', None, 'tp'), may hold values from -0.125 to 0.125
- up_weight: bfloat16 [8, 2048, 4096], P('ep', None, 'tp'), may hold values from -0.125 to 0.125
- down_weight: bfloat16 [8, 4096, 2048], P('ep', 'tp'), may hold values from -0.09375 to 0.09375
Outputs:
- combined: bfloat16 [2048, 2048], P('ep', 'tp')
Inputs may be any that keep to these rules, and one draw needn't show every extreme that they name: Each row of chosen lists 256 distinct token numbers in ascending order. Of the 256 consecutive tokens of one index of ep, a row holds at most 48, and every draw has rows that hold exactly 48 of them.
All inputs are finite; a program needn't handle non-finite values.
Results may differ from a plain program's by a relative error of at most 0.02.
Values may be sent and summed in bfloat16 or wider, within the bound.
A program may use at most 64 MiB of HBM per device.

v0:
```python
import functools
import jax
import jax.numpy as jnp
from jax import lax
from jax.experimental import pallas as pl
from jax.experimental.pallas import tpu as pltpu
from jax.sharding import PartitionSpec as P

F32 = jnp.float32
BF16 = jnp.bfloat16
MESH = pl.DeviceIdType.MESH
SHARES = (1, 1, 1)
CUTS_IN = ((1, 1), (1, 1), (1, 1))
CUTS_OUT = ((1,), (1,), (1,))
CUTS_BACK = ((1, 1), (1, 1), (1, 1))

def shards(tokens, norm_gain, chosen, route_weight, gate_weight, up_weight, down_weight):
    tok_rows, row_width = tokens.shape
    experts, capacity = chosen.shape
    ep_count = lax.axis_size("ep")
    tp_count = lax.axis_size("tp")
    owner_index = lax.axis_index("ep")
    slot_most = 3 * tok_rows // 16
    col_width = row_width // tp_count
    values = tokens.astype(jnp.float32)
    scale = lax.rsqrt(jnp.mean(values * values, axis=-1, keepdims=True) + 1e-06)
    normed = (values * scale * norm_gain[None, :]).astype(jnp.bfloat16)
    slot_steps = jnp.arange(slot_most, dtype=jnp.int32)
    first_token = owner_index * tok_rows
    run_start = jnp.sum((chosen < first_token).astype(jnp.int32), axis=1)
    run_end = jnp.sum((chosen < first_token + tok_rows).astype(jnp.int32), axis=1)
    run_count = run_end - run_start
    slot_live = slot_steps[None, :] < run_count[:, None]
    slot_place = jnp.minimum(run_start[:, None] + slot_steps[None, :], capacity - 1)
    slot_token = jnp.take_along_axis(chosen, slot_place, axis=1) - first_token
    slot_local = jnp.where(slot_live, slot_token, 0)
    my_chosen = lax.dynamic_index_in_dim(chosen, owner_index, 0, keepdims=False)
    block_edges = jnp.arange(ep_count, dtype=jnp.int32) * tok_rows
    src_start = jnp.sum((my_chosen[None, :] < block_edges[:, None]).astype(jnp.int32), axis=1)
    src_end = jnp.concatenate([src_start[1:], jnp.full((1,), capacity, jnp.int32)])
    gate_mat = gate_weight[0]
    up_mat = up_weight[0]
    down_mat = down_weight[0]
    outgoing = jnp.where(slot_live[:, :, None], normed[slot_local], jnp.zeros((), jnp.bfloat16))
    received = lax.all_to_all(outgoing, "ep", split_axis=0, concat_axis=0, tiled=True)
    source_block = my_chosen // tok_rows
    flat_index = (
        source_block * slot_most + jnp.arange(capacity, dtype=jnp.int32) - src_start[source_block]
    )
    expert_rows = received.reshape(-1, row_width)[flat_index]
    gate_pre = jnp.dot(expert_rows, gate_mat, preferred_element_type=jnp.float32)
    up_pre = jnp.dot(expert_rows, up_mat, preferred_element_type=jnp.float32)
    hidden = (jax.nn.silu(gate_pre) * up_pre).astype(jnp.bfloat16)
    summed_out = lax.psum_scatter(
        lax.dot_general(
            down_mat, hidden, (((0,), (1,)), ((), ())), preferred_element_type=jnp.float32
        ).astype(jnp.bfloat16),
        "tp",
        scatter_dimension=0,
        tiled=True,
    ).astype(jnp.float32)
    weighted = (summed_out.T * route_weight[0][:, None]).astype(jnp.bfloat16)
    back_place = jnp.minimum(src_start[:, None] + slot_steps[None, :], capacity - 1)
    back_live = slot_steps[None, :] < (src_end - src_start)[:, None]
    outgoing_back = jnp.where(
        back_live[:, :, None], weighted[back_place], jnp.zeros((), jnp.bfloat16)
    )
    returned = lax.all_to_all(outgoing_back, "ep", split_axis=0, concat_axis=0, tiled=True)
    target_row = jnp.where(slot_live, slot_token, tok_rows).reshape(-1)
    placement = (jnp.arange(tok_rows, dtype=jnp.int32)[:, None] == target_row[None, :]).astype(
        jnp.bfloat16
    )
    combined = jnp.dot(
        placement, returned.reshape(-1, col_width), preferred_element_type=jnp.float32
    )
    return combined.astype(jnp.bfloat16)


def cut(total, shares):
    sizes = [total * s // sum(shares) for s in shares]
    return [(sum(sizes[:i]), size) for i, size in enumerate(sizes)]


def group_rows(cap, slots, ep, first, count):
    most = max(min(m * count, cap - m * first) for m in range(1, ep + 1))
    return min(-(-most // 16) * 16, ep * count)


def fused_kernel(
    ep, groups, rows_of, cuts_in, cuts_out, cuts_back,
    tokens_hbm, gain_hbm, chosen_hbm, route_hbm, gate_hbm, up_hbm, down_hbm, out,
    tokens, gain, chosen, route,
    gate_w, up_w, down_w, normed, pick, unpick, spread, gather, weight, gate_acc, up_acc, hidden,
    outgoing, received, rows, pair_out, pair_in, own_part, cross_out, cross_in, back_out, back_in, done,
    in_sem, w_sem, send_sem, ep_recv, y_recv, pair_recv, relay_recv, ps_recv, ys_recv, back_recv,
):
    me = lax.axis_index("ep")
    tp = lax.axis_index("tp")
    y_pos = tp // 2
    core = tp % 2
    mate = y_pos * 2 + (1 - core)
    across = (1 - y_pos) * 2 + core
    diag = (1 - y_pos) * 2 + (1 - core)
    tok_rows, width = tokens.shape
    cap = chosen.shape[1]
    quarter = width // 4
    ff = gate_w.shape[1]
    n_groups = len(groups)
    slots = sum(n for _, n in groups)

    if ep & (ep - 1):
        peers = [(me + d) % ep for d in sorted(range(1, ep), key=lambda d: abs(d - ep / 2))]
    else:
        bits = [1 << i for i in range(ep.bit_length() - 1)]

        def flip(mask):
            dest = me
            for b in bits:
                if mask & b:
                    dest = dest + b * (1 - 2 * (me // b % 2))
            return dest

        peers = [flip(m) for m in range(ep - 1, 0, -1)]

    small = [
        pltpu.make_async_copy(a, b, in_sem.at[i])
        for i, (a, b) in enumerate(
            [(chosen_hbm, chosen), (tokens_hbm, tokens), (gain_hbm, gain), (route_hbm, route)]
        )
    ]
    for load in small:
        load.start()
    barrier = pltpu.get_barrier_semaphore()
    for dest in peers:
        pl.semaphore_signal(barrier, inc=1, device_id={"ep": dest, "tp": tp}, device_id_type=MESH)
    for other in (mate, across):
        pl.semaphore_signal(barrier, inc=1, device_id={"ep": me, "tp": other}, device_id_type=MESH)

    loads = [
        pltpu.make_async_copy(gate_hbm.at[0], gate_w, w_sem.at[0]),
        pltpu.make_async_copy(up_hbm.at[0], up_w, w_sem.at[1]),
        pltpu.make_async_copy(down_hbm.at[0], down_w, w_sem.at[2]),
    ]
    small[0].wait()

    first = me * tok_rows
    lane = lax.broadcasted_iota(jnp.int32, (slots, cap), 1).astype(F32)
    sub = lax.broadcasted_iota(jnp.int32, (slots, cap), 0).astype(F32)
    tok_lane = lax.broadcasted_iota(jnp.int32, (slots, tok_rows), 1).astype(F32)
    for e in range(ep):
        row = chosen[e : e + 1, :]
        local = (row - first).astype(F32)
        start = jnp.sum(jnp.where(local < 0.0, 1.0, 0.0), axis=1, keepdims=True)
        value = jnp.where((local >= 0.0) & (local < float(tok_rows)), local + 1.0, 0.0)
        hit = lane == sub + start
        slot_tok = jnp.sum(jnp.where(hit, value, 0.0), axis=1, keepdims=True) - 1.0
        one = jnp.where(tok_lane == slot_tok, 1.0, 0.0)
        for g, (s0, n) in enumerate(groups):
            pick[g][e * n : (e + 1) * n, :] = one[s0 : s0 + n]

    for load in small[1:]:
        load.wait()
    my_cols = pl.ds(pl.multiple_of(tp * quarter, quarter), quarter)
    my_gain = gain[:, my_cols]
    step_rows = 32
    for r in range(0, tok_rows, step_rows):
        rs = pl.ds(r, step_rows)
        v = tokens[rs, :].astype(F32)
        scale = lax.rsqrt(jnp.sum(v * v, axis=1, keepdims=True) * (1.0 / width) + 1e-06)
        own = tokens[rs, my_cols].astype(F32)
        normed[rs, :] = (own * scale * my_gain).astype(BF16)

    def ep_copies(buf_out, buf_in, n, r_sem):
        return [
            pltpu.make_async_remote_copy(
                src_ref=buf_out.at[pl.ds(pl.multiple_of(dest * n, 8), n)],
                dst_ref=buf_in.at[pl.ds(pl.multiple_of(me * n, 8), n)],
                send_sem=send_sem.at[0], recv_sem=r_sem,
                device_id={"ep": dest, "tp": tp}, device_id_type=MESH,
            )
            for dest in peers
        ]

    def tp_copy(a, b, r_sem, other):
        return pltpu.make_async_remote_copy(
            src_ref=a, dst_ref=b, send_sem=send_sem.at[0], recv_sem=r_sem,
            device_id={"ep": me, "tp": other}, device_id_type=MESH,
        )

    sent = []

    def go(c, size):
        c.start()
        sent.append(size)

    def landed(buf, n, sem):
        part = buf.at[pl.ds(0, n)]
        pltpu.make_async_copy(part, part, sem).wait()

    def mine_rows(n):
        return pl.ds(pl.multiple_of(me * n, 8), n)

    def send_in(g, k):
        n = groups[g][1]
        off, size = cuts_in[g][k]
        got = jnp.dot(
            pick[g][...].astype(BF16), normed[:, off : off + size], preferred_element_type=F32
        )
        outgoing[g][k][...] = got.astype(BF16)

    def start_in(g, k):
        n = groups[g][1]
        for c in ep_copies(outgoing[g][k], received[g][k], n, ep_recv[g].at[k]):
            go(c, n * cuts_in[g][k][1])
        received[g][k][mine_rows(n), :] = outgoing[g][k][mine_rows(n), :]

    send_in(0, 0)
    pl.semaphore_wait(barrier, ep + 1)
    start_in(0, 0)
    for k in range(1, len(cuts_in[0])):
        send_in(0, k)
        start_in(0, k)
    for load in loads:
        load.start()

    for g in range(1, n_groups):
        for k in range(len(cuts_in[g])):
            send_in(g, k)

    mine = chosen[pl.ds(me, 1), :].astype(F32)
    place = lax.broadcasted_iota(jnp.int32, (1, cap), 1).astype(F32)
    rank = jnp.zeros((1, cap), F32)
    block = jnp.zeros((1, cap), F32)
    edges = [(mine >= float(b * tok_rows)) & (mine < float((b + 1) * tok_rows)) for b in range(ep)]
    for b in range(ep):
        begin = jnp.sum(jnp.where(mine < float(b * tok_rows), 1.0, 0.0), axis=1, keepdims=True)
        rank = jnp.where(edges[b], place - begin, rank)
        block = jnp.where(edges[b], float(b), block)
    for g, (s0, n) in enumerate(groups):
        inside = (rank >= float(s0)) & (rank < float(s0 + n))
        slot_of = jnp.where(inside, block * float(n) + rank - float(s0), -1.0)
        slot_sub = lax.broadcasted_iota(jnp.int32, (ep * n, cap), 0).astype(F32)
        slot_hot = slot_sub == slot_of
        if rows_of[g] == ep * n:
            row_hot = slot_hot
        else:
            row_id = jnp.zeros((1, cap), F32)
            for b in range(ep):
                below = jnp.where(inside & (mine < float(b * tok_rows)), 1.0, 0.0)
                shift = jnp.sum(below, axis=1, keepdims=True) - float(s0)
                row_id = jnp.where(edges[b], rank + shift, row_id)
            row_id = jnp.where(inside, row_id, -1.0)
            row_sub = lax.broadcasted_iota(jnp.int32, (rows_of[g], cap), 0).astype(F32)
            row_hot = row_sub == row_id
            slot_b = jnp.where(slot_hot, 1.0, 0.0).astype(BF16)
            row_b = jnp.where(row_hot, 1.0, 0.0).astype(BF16)
            across_lanes = (((1,), (1,)), ((), ()))
            spread[g][...] = lax.dot_general(
                slot_b, row_b, across_lanes, preferred_element_type=F32
            ).astype(BF16)
            gather[g][...] = lax.dot_general(
                row_b, slot_b, across_lanes, preferred_element_type=F32
            ).astype(BF16)
        weight[g][...] = jnp.sum(jnp.where(row_hot, route[...], 0.0), axis=1, keepdims=True)
        unpick[g][...] = pick[g][...].T.astype(BF16)

    def start_on(side, *chunks):
        @pl.when(core == side)
        def _():
            for g, k in chunks:
                n = groups[g][1]
                for c in ep_copies(outgoing[g][k], received[g][k], n, ep_recv[g].at[k]):
                    c.start()
                    if side:
                        sent.append(n * cuts_in[g][k][1])
                received[g][k][mine_rows(n), :] = outgoing[g][k][mine_rows(n), :]

    def recv(g, k):
        n = groups[g][1]
        landed(received[g][k], (ep - 1) * n, ep_recv[g].at[k])
        mine_k = rows[g][k].at[tp]
        if rows_of[g] == ep * n:
            mine_k[...] = received[g][k][...]
        else:
            got = jnp.dot(gather[g][...], received[g][k][...], preferred_element_type=F32)
            mine_k[...] = got.astype(BF16)
        size = rows_of[g] * cuts_in[g][k][1]
        go(tp_copy(mine_k, mine_k, y_recv[g].at[k], across), size)
        go(tp_copy(mine_k, mine_k, pair_recv[g].at[k], mate), size)

    def relay(g, k):
        there = rows[g][k].at[across]
        tp_copy(there, there, y_recv[g].at[k], across).wait_recv()
        go(tp_copy(there, there, relay_recv[g].at[k], mate), rows_of[g] * cuts_in[g][k][1])

    def project(g, near, far, opening=False, closing=False):
        for k in near:
            there = rows[g][k].at[mate]
            tp_copy(there, there, pair_recv[g].at[k], mate).wait_recv()
        for k in far:
            there = rows[g][k].at[diag]
            tp_copy(there, there, relay_recv[g].at[k], mate).wait_recv()
        work = [(k, t) for k in near for t in (tp, mate)] + [(k, t) for k in far for t in (across, diag)]
        tile = 256
        for n in range(0, ff, tile):
            cols = pl.ds(n, tile)
            gg = None if opening else gate_acc[g][:, cols]
            uu = None if opening else up_acc[g][:, cols]
            for k, t in work:
                off, size = cuts_in[g][k]
                ks = pl.ds(pl.multiple_of(t * quarter + off, 128), size)
                x = rows[g][k][t]
                dg = jnp.dot(x, gate_w[ks, cols], preferred_element_type=F32)
                du = jnp.dot(x, up_w[ks, cols], preferred_element_type=F32)
                gg = dg if gg is None else gg + dg
                uu = du if uu is None else uu + du
            if closing:
                hidden[g][:, cols] = (gg / (1.0 + jnp.exp(-gg)) * uu).astype(BF16)
            else:
                gate_acc[g][:, cols] = gg
                up_acc[g][:, cols] = uu

    def down(g, t, j):
        off, size = cuts_out[g][j]
        cols = pl.ds(pl.multiple_of(t * quarter + off, 128), size)
        return jnp.dot(hidden[g][...], down_w[:, cols], preferred_element_type=F32)

    def pair_copy(g, j, half):
        return tp_copy(pair_out[g][j].at[half], pair_in[g][j].at[half], ps_recv[g].at[j, half], mate)

    def give(g, j):
        for half, t in enumerate((diag, mate)):
            pair_out[g][j][half] = down(g, t, j).astype(BF16)
            go(pair_copy(g, j, half), rows_of[g] * cuts_out[g][j][1])

    def keep(g, j, which):
        own_part[g][j][which] = down(g, tp if which else across, j)

    def piece(g, i):
        off, size = cuts_back[g][i]
        for j, (base, wide) in enumerate(cuts_out[g]):
            if base <= off < base + wide:
                return j, slice(off - base, off - base + size)

    def cross(g, i):
        j, part = piece(g, i)
        if part.start == 0:
            pair_copy(g, j, 0).wait_recv()
        kept = own_part[g][j][0, :, part] + pair_in[g][j][0, :, part].astype(F32)
        cross_out[g][i][...] = kept.astype(BF16)
        go(tp_copy(cross_out[g][i], cross_in[g][i], ys_recv[g].at[i], across), rows_of[g] * cuts_back[g][i][1])

    def back(g, i):
        n = groups[g][1]
        j, part = piece(g, i)
        if part.start == 0:
            pair_copy(g, j, 1).wait_recv()
        near = own_part[g][j][1, :, part] + pair_in[g][j][1, :, part].astype(F32)
        tp_copy(cross_out[g][i], cross_in[g][i], ys_recv[g].at[i], across).wait_recv()
        total = ((near + cross_in[g][i][...].astype(F32)) * weight[g][...]).astype(BF16)
        if rows_of[g] == ep * n:
            back_out[g][i][...] = total
        else:
            wide = jnp.dot(spread[g][...], total, preferred_element_type=F32)
            back_out[g][i][...] = wide.astype(BF16)
        for c in ep_copies(back_out[g][i], back_in[g][i], n, back_recv[g].at[i]):
            go(c, n * cuts_back[g][i][1])
        back_in[g][i][mine_rows(n), :] = back_out[g][i][mine_rows(n), :]

    def finish(g, i):
        n = groups[g][1]
        off, size = cuts_back[g][i]
        landed(back_in[g][i], (ep - 1) * n, back_recv[g].at[i])
        part = jnp.dot(unpick[g][...], back_in[g][i][...], preferred_element_type=F32)
        if g:
            part = part + done[:, off : off + size]
        if g == n_groups - 1:
            out[:, off : off + size] = part.astype(BF16)
        else:
            done[:, off : off + size] = part

    def weights(i):
        loads[i].wait()

    start_on(0, (1, 0), (1, 1))
    recv(0, 0)
    start_on(1, (1, 0), (1, 1))
    recv(0, 1)
    start_on(0, (2, 0), (2, 1))
    weights(0)
    weights(1)
    project(0, [0, 1], [], opening=True)
    recv(1, 0)
    start_on(1, (2, 0), (2, 1))
    relay(0, 0)
    recv(1, 1)
    relay(0, 1)
    project(0, [], [0, 1], closing=True)
    weights(2)
    give(0, 0)
    recv(2, 0)
    relay(1, 0)
    keep(0, 0, 0)
    recv(2, 1)
    relay(1, 1)
    project(1, [1], [], opening=True)
    cross(0, 0)
    project(1, [0], [0])
    cross(0, 1)
    project(1, [], [1], closing=True)
    give(1, 0)
    relay(2, 1)
    relay(2, 0)
    keep(0, 0, 1)
    keep(1, 0, 1)
    project(2, [0], [], opening=True)
    keep(1, 0, 0)
    cross(1, 0)
    cross(1, 1)
    project(2, [], [0])
    back(0, 0)
    project(2, [1], [1], closing=True)
    give(2, 0)
    back(0, 1)
    keep(2, 0, 0)
    cross(2, 0)
    back(1, 0)
    back(1, 1)
    keep(2, 0, 1)
    finish(0, 0)
    cross(2, 1)
    finish(0, 1)
    back(2, 0)
    back(2, 1)
    finish(1, 0)
    finish(1, 1)
    finish(2, 0)
    finish(2, 1)

    words = sum(sent)
    rest = pl.ds(0, words // ff)
    pltpu.make_async_copy(gate_w.at[rest], gate_w.at[rest], send_sem.at[0]).wait()


def fused(tokens, norm_gain, chosen, route_weight, gate_weight, up_weight, down_weight):
    ep = lax.axis_size("ep")
    tok_rows, width = tokens.shape
    cap = chosen.shape[1]
    slots = 3 * tok_rows // 16
    quarter = width // lax.axis_size("tp")
    ff = gate_weight.shape[2]
    groups = cut(slots, SHARES)
    rows_of = [group_rows(cap, slots, ep, s0, n) for s0, n in groups]
    cuts_in = [cut(quarter, c) for c in CUTS_IN]
    cuts_out = [cut(quarter, c) for c in CUTS_OUT]
    cuts_back = [cut(quarter, c) for c in CUTS_BACK]
    hbm = pl.BlockSpec(memory_space=pl.ANY)
    dma = pltpu.SemaphoreType.DMA
    wide = [ep * n for _, n in groups]

    def bufs(cuts, lead, dtype=BF16):
        return [[pltpu.VMEM(lead(g) + (size,), dtype) for _, size in c] for g, c in enumerate(cuts)]

    def each(shape, dtype=BF16):
        return [pltpu.VMEM(shape(g), dtype) for g in range(len(groups))]

    def sems(cuts):
        return [dma((len(c),)) for c in cuts]

    return pl.pallas_call(
        functools.partial(fused_kernel, ep, groups, rows_of, cuts_in, cuts_out, cuts_back),
        out_shape=pltpu.VMEM((tok_rows, quarter), BF16),
        in_specs=[hbm] * 7,
        out_specs=pl.BlockSpec(memory_space=pltpu.VMEM),
        scratch_shapes=[
            pltpu.VMEM((tok_rows, width), BF16),
            pltpu.VMEM((1, width), F32),
            pltpu.VMEM(chosen.shape, jnp.int32),
            pltpu.VMEM((1, cap), F32),
            pltpu.VMEM((width, ff), BF16),
            pltpu.VMEM((width, ff), BF16),
            pltpu.VMEM((ff, width), BF16),
            pltpu.VMEM((tok_rows, quarter), BF16),
            each(lambda g: (wide[g], tok_rows), F32),
            each(lambda g: (tok_rows, wide[g])),
            each(lambda g: (wide[g], rows_of[g])),
            each(lambda g: (rows_of[g], wide[g])),
            each(lambda g: (rows_of[g], 1), F32),
            each(lambda g: (rows_of[g], ff), F32),
            each(lambda g: (rows_of[g], ff), F32),
            each(lambda g: (rows_of[g], ff)),
            bufs(cuts_in, lambda g: (wide[g],)),
            bufs(cuts_in, lambda g: (wide[g],)),
            bufs(cuts_in, lambda g: (4, rows_of[g])),
            bufs(cuts_out, lambda g: (2, rows_of[g])),
            bufs(cuts_out, lambda g: (2, rows_of[g])),
            bufs(cuts_out, lambda g: (2, rows_of[g]), F32),
            bufs(cuts_back, lambda g: (rows_of[g],)),
            bufs(cuts_back, lambda g: (rows_of[g],)),
            bufs(cuts_back, lambda g: (wide[g],)),
            bufs(cuts_back, lambda g: (wide[g],)),
            pltpu.VMEM((tok_rows, quarter), F32),
            dma((4,)),
            dma((3,)),
            dma((1,)),
            sems(cuts_in),
            sems(cuts_in),
            sems(cuts_in),
            sems(cuts_in),
            [dma((len(c), 2)) for c in cuts_out],
            sems(cuts_back),
            sems(cuts_back),
        ],
        compiler_params=pltpu.CompilerParams(
            collective_id=0, has_side_effects=True, vmem_limit_bytes=60 * 1024 * 1024
        ),
    )(tokens, norm_gain[None, :], chosen, route_weight, gate_weight, up_weight, down_weight)


def solution(mesh):
    small = mesh.shape["tp"] == 4
    return jax.shard_map(
        fused if small else shards,
        mesh=mesh,
        in_specs=(
            P("ep", None),
            P(),
            P(),
            P("ep", None),
            P("ep", None, "tp"),
            P("ep", None, "tp"),
            P("ep", "tp", None),
        ),
        out_specs=P("ep", "tp"),
        check_vma=False,
    )
```

profile of v0, /device:TPU:0, one launch (start us, length us, event | category | flops | bytes accessed | tf_op | source)
XLA Modules:
  0.0 35.2 jit_solution(3956524525605708004)
XLA Ops:
  0.0 34.5 %shard_map.73 = bf16[256,512]{1,0:T(8,128)(2,1)S(1)} custom-call(bf16[256,2048]{1,0:T(8,128)(2,1)} %tokens_hbm.1, f32[1,2048]{1,0:T(1,128)} %bitcast.1, s32[8,256]{1,0:T(8,128)} %chosen_hbm.1, f32[1,256]{1,0:T(1,128)} %route_hbm.1, bf16[1,2048,1024]{2,1,0:T(8,128)(2,1)} %gate_hbm.1, bf16[1,2048,1024]{2,1,0:T(8,128)(2,1)} %up_hbm.1, ...), custom_call_target="tpu_custom_call" | custom-call | tf_op jit(solution)/shard_map/pallas_call | solution.py:470
  34.5 0.7 %copy.9 = bf16[256,512]{1,0:T(8,128)(2,1)} copy(bf16[256,512]{1,0:T(8,128)(2,1)S(1)} %shard_map.73) | data formatting | bytes 524288
where the time goes:
time: 35.4 us; the launch traced here: 35.2 us
  Pallas kernels  34.5 us (97%)
  local copies, waits for them, and re-layouts  0.71 us (2%)
    pallas_call x1, Pallas kernels, fused(): pl.pallas_call(functools.partial(fused_kernel, ep, groups, rows_of, cuts_...  34.5 us

commit v1 on v0

--- a/solution.py
+++ b/solution.py
@@ -122,10 +122,17 @@
 
         peers = [flip(m) for m in range(ep - 1, 0, -1)]
 
+    top_half, low_half = pl.ds(0, tok_rows // 2), pl.ds(tok_rows // 2, tok_rows // 2)
     small = [
         pltpu.make_async_copy(a, b, in_sem.at[i])
         for i, (a, b) in enumerate(
-            [(chosen_hbm, chosen), (tokens_hbm, tokens), (gain_hbm, gain), (route_hbm, route)]
+            [
+                (chosen_hbm, chosen),
+                (tokens_hbm.at[top_half], tokens.at[top_half]),
+                (gain_hbm, gain),
+                (tokens_hbm.at[low_half], tokens.at[low_half]),
+                (route_hbm, route),
+            ]
         )
     ]
     for load in small:
@@ -158,12 +165,15 @@
         for g, (s0, n) in enumerate(groups):
             pick[g][e * n : (e + 1) * n, :] = one[s0 : s0 + n]
 
-    for load in small[1:]:
+    for load in small[1:3]:
         load.wait()
     my_cols = pl.ds(pl.multiple_of(tp * quarter, quarter), quarter)
     my_gain = gain[:, my_cols]
     step_rows = 32
     for r in range(0, tok_rows, step_rows):
+        if r == tok_rows // 2:
+            for load in small[3:]:
+                load.wait()
         rs = pl.ds(r, step_rows)
         v = tokens[rs, :].astype(F32)
         scale = lax.rsqrt(jnp.sum(v * v, axis=1, keepdims=True) * (1.0 / width) + 1e-06)
@@ -329,12 +339,15 @@
         return tp_copy(pair_out[g][j].at[half], pair_in[g][j].at[half], ps_recv[g].at[j, half], mate)
 
     def give(g, j):
-        for half, t in enumerate((diag, mate)):
-            pair_out[g][j][half] = down(g, t, j).astype(BF16)
+        parts = [down(g, t, j) for t in (diag, mate)]
+        for half, part in enumerate(parts):
+            pair_out[g][j][half] = part.astype(BF16)
             go(pair_copy(g, j, half), rows_of[g] * cuts_out[g][j][1])
 
-    def keep(g, j, which):
-        own_part[g][j][which] = down(g, tp if which else across, j)
+    def keep(g, j):
+        parts = [down(g, t, j) for t in (across, tp)]
+        for which, part in enumerate(parts):
+            own_part[g][j][which] = part
 
     def piece(g, i):
         off, size = cuts_back[g][i]
@@ -389,49 +402,46 @@
     start_on(0, (2, 0), (2, 1))
     weights(0)
     weights(1)
-    project(0, [0, 1], [], opening=True)
+    project(0, [1], [], opening=True)
     recv(1, 0)
     start_on(1, (2, 0), (2, 1))
+    project(0, [0], [])
+    recv(1, 1)
     relay(0, 0)
-    recv(1, 1)
     relay(0, 1)
+    project(1, [0], [], opening=True)
     project(0, [], [0, 1], closing=True)
+    recv(2, 0)
     weights(2)
     give(0, 0)
-    recv(2, 0)
+    recv(2, 1)
     relay(1, 0)
-    keep(0, 0, 0)
-    recv(2, 1)
+    keep(0, 0)
     relay(1, 1)
-    project(1, [1], [], opening=True)
     cross(0, 0)
-    project(1, [0], [0])
+    project(1, [1], [0])
     cross(0, 1)
     project(1, [], [1], closing=True)
     give(1, 0)
     relay(2, 1)
     relay(2, 0)
-    keep(0, 0, 1)
-    keep(1, 0, 1)
-    project(2, [0], [], opening=True)
-    keep(1, 0, 0)
+    project(2, [1], [], opening=True)
+    keep(1, 0)
     cross(1, 0)
     cross(1, 1)
-    project(2, [], [0])
     back(0, 0)
-    project(2, [1], [1], closing=True)
+    project(2, [0], [0, 1], closing=True)
     give(2, 0)
     back(0, 1)
-    keep(2, 0, 0)
+    keep(2, 0)
     cross(2, 0)
     back(1, 0)
     back(1, 1)
-    keep(2, 0, 1)
-    finish(0, 0)
     cross(2, 1)
-    finish(0, 1)
     back(2, 0)
     back(2, 1)
+    finish(0, 0)
+    finish(0, 1)
     finish(1, 0)
     finish(1, 1)
     finish(2, 0)
@@ -500,7 +510,7 @@
             bufs(cuts_back, lambda g: (wide[g],)),
             bufs(cuts_back, lambda g: (wide[g],)),
             pltpu.VMEM((tok_rows, quarter), F32),
-            dma((4,)),
+            dma((5,)),
             dma((3,)),
             dma((1,)),
             sems(cuts_in),

time: 35.4 us -> 34.7 us (0.980)
  Pallas kernels: 34.5 us -> 33.8 us
    pallas_call x1, Pallas kernels: 34.5 us -> 33.8 us  [fused(): pl.pallas_call(functools.partial(fused_kernel, ep, groups, rows_of, cuts_...]
where the time goes in v1:
time: 34.7 us; the launch traced here: 34.5 us
  Pallas kernels  33.8 us (97%)
  local copies, waits for them, and re-layouts  0.71 us (2%)
    pallas_call x1, Pallas kernels, fused(): pl.pallas_call(functools.partial(fused_kernel, ep, groups, rows_of, cuts_...  33.8 us
    unnamed x1, local copies, waits for them, and re-layouts  0.71 us

profile of v1, /device:TPU:0, one launch (start us, length us, event | category | flops | bytes accessed | tf_op | source)
XLA Modules:
  0.0 34.5 jit_solution(2345214040669061909)
XLA Ops:
  0.0 33.8 %shard_map.73 = bf16[256,512]{1,0:T(8,128)(2,1)S(1)} custom-call(bf16[256,2048]{1,0:T(8,128)(2,1)} %tokens_hbm.1, f32[1,2048]{1,0:T(1,128)} %bitcast.1, s32[8,256]{1,0:T(8,128)} %chosen_hbm.1, f32[1,256]{1,0:T(1,128)} %route_hbm.1, bf16[1,2048,1024]{2,1,0:T(8,128)(2,1)} %gate_hbm.1, bf16[1,2048,1024]{2,1,0:T(8,128)(2,1)} %up_hbm.1, ...), custom_call_target="tpu_custom_call" | custom-call | tf_op jit(solution)/shard_map/pallas_call | solution.py:480
  33.8 0.7 %copy.9 = bf16[256,512]{1,0:T(8,128)(2,1)} copy(bf16[256,512]{1,0:T(8,128)(2,1)S(1)} %shard_map.73) | data formatting | bytes 524288
